TPU v7x, 32 devices: a whole 2x2x4 slice. The times are simulated.
32 devices in a mesh: sp: 8 (over z, y), tp: 4 (over x, core).
Axes of the slice: x: 2, y: 2, z: 4, core: 2. Of those that a mesh axis runs over, the one named last changes fastest.
Arguments:
- residual_entry_input: bfloat16 [8192, 2048], P(('sp', 'tp')), may hold values from -6 to 6
- query_matrix_rows: bfloat16 [8192, 1024], P('sp', 'tp'), may hold values from -6 to 6
- key_matrix_rows: bfloat16 [8192, 1024], P('sp', 'tp'), may hold values from -6 to 6
- value_matrix_rows: bfloat16 [8192, 2048], P('sp', 'tp'), may hold values from -6 to 6
- output_gate_logits: bfloat16 [8192, 2048], P('sp', 'tp'), may hold values from -6 to 6
- input_gate_logits: float32 [8192, 8], P('sp', 'tp'), may hold values from -6 to 6
- forget_gate_logits: float32 [8192, 8], P('sp', 'tp'), may hold values from -8 to 31
- forget_decay_offset: float32 [8192, 8], P('sp', 'tp'), may hold values from -0.7 to 0
- head_norm_gain: float32 [8, 256], P('tp'), may hold values from 0.1 to 1.9
- cell_output_weight: bfloat16 [2048, 2048], P('tp'), may hold values from -0.125 to 0.125
- feedforward_norm_gain: float32 [2048], replicated, may hold values from 0.1 to 1.9
- gate_up_weight: bfloat16 [2048, 5632], P('sp', 'tp'), may hold values from -0.125 to 0.125
- value_up_weight: bfloat16 [2048, 5632], P('sp', 'tp'), may hold values from -0.125 to 0.125
- gate_filter_taps: float32 [3, 5632], P(None, 'tp'), may hold values from -3 to 3
- value_filter_taps: float32 [3, 5632], P(None, 'tp'), may hold values from -3 to 3
- down_projection_weight: bfloat16 [5632, 2048], P('tp', 'sp'), may hold values from -0.078125 to 0.078125
Outputs:
- result: bfloat16 [8192, 2048], P(('sp', 'tp'))
All inputs are finite; a program needn't handle non-finite values.
Results may differ from a plain program's by a relative error of at most 0.025.
Values may be sent and summed in bfloat16 or wider, within the bound.
No kernel may reach another device: no remote copies, remote signals or barrier semaphores. Data moves between devices by JAX's collectives and lax.ppermute only.
A program may use at most 128 MiB of HBM per device.

v0:
```python
import jax
import jax.numpy as jnp
from jax import lax
from jax.sharding import PartitionSpec as P

BLOCK = 128
eps = 1e-06
neg_large = -1e30


def carried_in(x, axis, combine, identity):
    count, position = (lax.axis_size(axis), lax.axis_index(axis))
    everything = jax.tree.map(
        lambda part, kind: lax.all_gather(part.astype(kind), axis),
        x,
        (jnp.bfloat16, jnp.bfloat16, jnp.bfloat16, jnp.bfloat16),
    )
    start = jax.tree.map(
        lambda part, zero: jnp.broadcast_to(jnp.asarray(zero, part.dtype), part.shape), x, identity
    )

    def lap(k, before):
        reached = k < position
        new = combine(
            before, jax.tree.map(lambda part, own: part[k].astype(own.dtype), everything, x)
        )
        return jax.tree.map(lambda a, b: jnp.where(reached, a, b), new, before)

    return lax.fori_loop(0, count, lap, start)


def shifted(x, axis, by):
    count = lax.axis_size(axis)
    pairs = [(i, i + by) for i in range(count) if 0 <= i + by < count]
    return lax.ppermute(x, axis, pairs)


def gate_log_values(input_gate_logits, forget_gate_logits, forget_decay_offset):
    input_log_value = 15.0 * jnp.tanh(input_gate_logits / 15.0)
    forget_log_sigmoid = (
        jax.nn.log_sigmoid(15.0 * jnp.tanh(forget_gate_logits / 15.0)) + forget_decay_offset
    )
    return (input_log_value, forget_log_sigmoid)


def combine_states(earlier, later):
    total_one, memory_one, normer_one, running_one = earlier
    total_two, memory_two, normer_two, running_two = later
    joined = jnp.maximum(total_two + running_one, running_two)
    weight_one = jnp.exp(total_two + running_one - joined)
    weight_two = jnp.exp(running_two - joined)
    memory = weight_one[:, None, None] * memory_one + weight_two[:, None, None] * memory_two
    normer = weight_one[:, None] * normer_one + weight_two[:, None] * normer_two
    return (total_one + total_two, memory, normer, joined)


def local_step(state_carry, inputs):
    memory, normer, running = state_carry
    query_block, key_block, value_block, input_block, forget_block = inputs
    length = query_block.shape[0]
    highest = lax.Precision.HIGHEST
    query_scale = query_block.shape[2] ** (-0.5)
    causal = jnp.tril(jnp.ones((length, length), dtype=bool))[:, :, None]
    cumulative = jnp.cumsum(forget_block, axis=0)
    logits = cumulative[:, None, :] - cumulative[None, :, :] + input_block[None, :, :]
    logits = jnp.where(causal, logits, -jnp.inf)
    carried = cumulative + running[None, :]
    stable = jnp.maximum(carried, jnp.max(logits, axis=1))
    carry_weight = jnp.exp(carried - stable)
    raw = (
        jnp.einsum("thd,shd->tsh", query_block, key_block, preferred_element_type=jnp.float32)
        * query_scale
    )
    scores = raw * jnp.exp(logits - stable[:, None, :])
    scaled_query = query_block.astype(jnp.float32) * query_scale
    numerator = carry_weight[:, :, None] * jnp.einsum(
        "hvd,thd->thv", memory, scaled_query, precision=highest
    )
    numerator = numerator + jnp.einsum(
        "tsh,shv->thv", scores.astype(jnp.bfloat16), value_block, preferred_element_type=jnp.float32
    )
    denominator = carry_weight * jnp.einsum(
        "hd,thd->th", normer, scaled_query, precision=highest
    ) + jnp.sum(scores, axis=1)
    last_sum = cumulative[-1]
    weights_log = last_sum[None, :] - cumulative + input_block
    new_running = jnp.maximum(last_sum + running, jnp.max(weights_log, axis=0))
    decay_factor = jnp.exp(last_sum + running - new_running)
    weighted = (
        key_block.astype(jnp.float32) * jnp.exp(weights_log - new_running[None, :])[:, :, None]
    )
    memory = decay_factor[:, None, None] * memory + jnp.einsum(
        "shv,shd->hvd",
        value_block,
        weighted.astype(jnp.bfloat16),
        preferred_element_type=jnp.float32,
    )
    normer = decay_factor[:, None] * normer + jnp.sum(weighted, axis=0)
    return ((memory, normer, new_running), (numerator, denominator, stable))


def local(
    residual_entry_input,
    query_matrix_rows,
    key_matrix_rows,
    value_matrix_rows,
    output_gate_logits,
    input_gate_logits,
    forget_gate_logits,
    forget_decay_offset,
    head_norm_gain,
    cell_output_weight,
    feedforward_norm_gain,
    gate_up_weight,
    value_up_weight,
    gate_filter_taps,
    value_filter_taps,
    down_projection_weight,
):
    highest = lax.Precision.HIGHEST
    token_count = query_matrix_rows.shape[0]
    head_count = input_gate_logits.shape[1]
    key_width = query_matrix_rows.shape[1] // head_count
    value_width = value_matrix_rows.shape[1] // head_count
    query_scale = key_width ** (-0.5)
    queries_low = query_matrix_rows.reshape(token_count, head_count, key_width)
    keys_low = key_matrix_rows.reshape(token_count, head_count, key_width)
    values_low = value_matrix_rows.reshape(token_count, head_count, value_width)
    input_log_value, forget_log_sigmoid = gate_log_values(
        input_gate_logits, forget_gate_logits, forget_decay_offset
    )
    cumulative = jnp.cumsum(forget_log_sigmoid, axis=0)
    total_log = cumulative[-1]
    block_count = token_count // BLOCK

    def blocks(tensor):
        return tensor.reshape((block_count, BLOCK) + tensor.shape[1:])

    initial = (
        jnp.zeros((head_count, value_width, key_width), jnp.float32),
        jnp.zeros((head_count, key_width), jnp.float32),
        jnp.full((head_count,), neg_large, jnp.float32),
    )
    end_state, (numerator, denominator, stable) = lax.scan(
        local_step,
        initial,
        (
            blocks(queries_low),
            blocks(keys_low),
            blocks(values_low),
            blocks(input_log_value),
            blocks(forget_log_sigmoid),
        ),
    )
    end_memory, end_normer, end_running = end_state
    identity = (
        jnp.zeros((head_count,), jnp.float32),
        jnp.zeros((head_count, value_width, key_width), jnp.float32),
        jnp.zeros((head_count, key_width), jnp.float32),
        jnp.full((head_count,), neg_large, jnp.float32),
    )
    prefix = carried_in(
        (total_log, end_memory, end_normer, end_running), "sp", combine_states, identity
    )
    numerator = numerator.reshape(token_count, head_count, value_width)
    denominator = denominator.reshape(token_count, head_count)
    stable = stable.reshape(token_count, head_count)
    _, prior_memory, prior_normer, prior_running = prefix
    scaled_query = queries_low.astype(jnp.float32) * query_scale
    prior_log = cumulative + prior_running[None, :]
    top_log = jnp.maximum(stable, prior_log)
    local_weight = jnp.exp(stable - top_log)
    prior_weight = jnp.exp(prior_log - top_log)
    numerator = local_weight[:, :, None] * numerator + prior_weight[:, :, None] * jnp.einsum(
        "hvd,thd->thv", prior_memory, scaled_query, precision=highest
    )
    denominator = local_weight * denominator + prior_weight * jnp.einsum(
        "hd,thd->th", prior_normer, scaled_query, precision=highest
    )
    memory_out = numerator / jnp.maximum(jnp.abs(denominator), jnp.exp(-top_log))[:, :, None]
    normed = (
        memory_out
        * lax.rsqrt(jnp.mean(memory_out * memory_out, axis=-1, keepdims=True) + eps)
        * head_norm_gain[None, :, :]
    )
    gated_rows = (
        normed.reshape(token_count, head_count * value_width)
        * jax.nn.sigmoid(output_gate_logits.astype(jnp.float32))
    ).astype(jnp.bfloat16)
    whole_out = lax.all_gather(cell_output_weight, "tp", axis=0, tiled=True)
    own_rows = lax.all_to_all(gated_rows, "tp", split_axis=0, concat_axis=1, tiled=True)
    mixed_rows = jnp.dot(own_rows, whole_out, preferred_element_type=jnp.float32)
    stream_wide = residual_entry_input.astype(jnp.float32) + mixed_rows
    stream = stream_wide.astype(jnp.bfloat16)
    stream_wide = lax.optimization_barrier(stream).astype(jnp.float32)
    normed_rows = (
        stream_wide
        * lax.rsqrt(jnp.mean(stream_wide * stream_wide, axis=-1, keepdims=True) + eps)
        * feedforward_norm_gain[None, :]
    ).astype(jnp.bfloat16)
    group_rows = lax.all_gather(normed_rows, "tp", axis=0, tiled=True)
    earlier_rows = shifted(group_rows[-2:], "sp", 1)
    window = jnp.concatenate([earlier_rows, group_rows], axis=0)
    up_gate = jnp.dot(
        window,
        lax.all_gather(gate_up_weight, "sp", axis=0, tiled=True),
        preferred_element_type=jnp.float32,
    )
    up_value = jnp.dot(
        window,
        lax.all_gather(value_up_weight, "sp", axis=0, tiled=True),
        preferred_element_type=jnp.float32,
    )
    conv_g = (
        gate_filter_taps[0][None, :] * up_gate[:-2]
        + gate_filter_taps[1][None, :] * up_gate[1:-1]
        + gate_filter_taps[2][None, :] * up_gate[2:]
    )
    conv_v = (
        value_filter_taps[0][None, :] * up_value[:-2]
        + value_filter_taps[1][None, :] * up_value[1:-1]
        + value_filter_taps[2][None, :] * up_value[2:]
    )
    hidden = (jax.nn.silu(conv_g) * conv_v).astype(jnp.bfloat16)
    whole_down = lax.all_gather(down_projection_weight, "sp", axis=1, tiled=True)
    ffn_rows = lax.psum_scatter(
        jnp.dot(hidden, whole_down, preferred_element_type=jnp.float32).astype(jnp.bfloat16),
        "tp",
        scatter_dimension=0,
        tiled=True,
    ).astype(jnp.float32)
    return (stream_wide + ffn_rows).astype(jnp.bfloat16)


def solution(mesh):
    in_specs = (
        P(("sp", "tp"), None),
        P("sp", "tp"),
        P("sp", "tp"),
        P("sp", "tp"),
        P("sp", "tp"),
        P("sp", "tp"),
        P("sp", "tp"),
        P("sp", "tp"),
        P("tp", None),
        P("tp", None),
        P(),
        P("sp", "tp"),
        P("sp", "tp"),
        P(None, "tp"),
        P(None, "tp"),
        P("tp", "sp"),
    )
    out_specs = P(("sp", "tp"), None)
    return jax.shard_map(local, mesh=mesh, in_specs=in_specs, out_specs=out_specs, check_vma=False)
```

profile of v0, /device:TPU:0, one launch (start us, length us, event | category | flops | bytes accessed | tf_op | source)
XLA Modules:
  0.0 629.0 jit_solution(18224603662122398015)
XLA Ops:
  7.6 1.3 reshape.215
  9.9 2.0 reshape.216
  12.8 105.2 %while.39 = (s32[]{:T(128)}, f32[2,256,128]{2,1,0:T(8,128)S(1)}, f32[2,128]{1,0:T(2,128)S(1)}, f32[2]{0:T(128)S(1)}, f32[8,128,2,256]{1,0,3,2:T(8,128)}, /*index...) while((s32[]{:T(128)}, f32[2,256,128]{2,1,0:T(8,128)S(1)}, ...), condition=%wide.region_6.7_spmd.clone, body=%wide.region_0.6_spmd.clone.sunk | while | flops 144166400 | bytes 4685610 | solution.py:144
  13.6 1.0 constant_dynamic-slice_fusion.10
  17.3 8.2 %dynamic_update_slice.19 = f32[8,128,2,256]{1,0,3,2:T(8,128)} dynamic-update-slice(f32[8,128,2,256]{1,0,3,2:T(8,128)} %get-tuple-element.661, f32[1,128,2,256]{1,0,3,2:T(1,128)S(1)} %copy.248, s32[]{:T(128)} %get-tuple-element.657, s32[]{:T(128)} %constant.83.clone.1..sunk, s32[]{:T(128)} %constant.83.clone.1..sunk, s32[]{:T(128)} %constant.83.clone.1..sunk) | dynamic-update-slice | bytes 524292 | tf_op jit(solution)/shard_map/while/body/jit(dynamic_update_index_in_dim)/dynamic_update_slice | solution.py:144
  26.7 1.0 constant_dynamic-slice_fusion.10
  30.5 8.2 %dynamic_update_slice.19 = f32[8,128,2,256]{1,0,3,2:T(8,128)} dynamic-update-slice(f32[8,128,2,256]{1,0,3,2:T(8,128)} %get-tuple-element.661, f32[1,128,2,256]{1,0,3,2:T(1,128)S(1)} %copy.248, s32[]{:T(128)} %get-tuple-element.657, s32[]{:T(128)} %constant.83.clone.1..sunk, s32[]{:T(128)} %constant.83.clone.1..sunk, s32[]{:T(128)} %constant.83.clone.1..sunk) | dynamic-update-slice | bytes 524292 | tf_op jit(solution)/shard_map/while/body/jit(dynamic_update_index_in_dim)/dynamic_update_slice | solution.py:144
  43.7 8.2 %dynamic_update_slice.19 = f32[8,128,2,256]{1,0,3,2:T(8,128)} dynamic-update-slice(f32[8,128,2,256]{1,0,3,2:T(8,128)} %get-tuple-element.661, f32[1,128,2,256]{1,0,3,2:T(1,128)S(1)} %copy.248, s32[]{:T(128)} %get-tuple-element.657, s32[]{:T(128)} %constant.83.clone.1..sunk, s32[]{:T(128)} %constant.83.clone.1..sunk, s32[]{:T(128)} %constant.83.clone.1..sunk) | dynamic-update-slice | bytes 524292 | tf_op jit(solution)/shard_map/while/body/jit(dynamic_update_index_in_dim)/dynamic_update_slice | solution.py:144
  53.0 1.0 constant_dynamic-slice_fusion.10
  56.8 8.2 %dynamic_update_slice.19 = f32[8,128,2,256]{1,0,3,2:T(8,128)} dynamic-update-slice(f32[8,128,2,256]{1,0,3,2:T(8,128)} %get-tuple-element.661, f32[1,128,2,256]{1,0,3,2:T(1,128)S(1)} %copy.248, s32[]{:T(128)} %get-tuple-element.657, s32[]{:T(128)} %constant.83.clone.1..sunk, s32[]{:T(128)} %constant.83.clone.1..sunk, s32[]{:T(128)} %constant.83.clone.1..sunk) | dynamic-update-slice | bytes 524292 | tf_op jit(solution)/shard_map/while/body/jit(dynamic_update_index_in_dim)/dynamic_update_slice | solution.py:144
  66.2 1.0 constant_dynamic-slice_fusion.10
  70.0 8.2 %dynamic_update_slice.19 = f32[8,128,2,256]{1,0,3,2:T(8,128)} dynamic-update-slice(f32[8,128,2,256]{1,0,3,2:T(8,128)} %get-tuple-element.661, f32[1,128,2,256]{1,0,3,2:T(1,128)S(1)} %copy.248, s32[]{:T(128)} %get-tuple-element.657, s32[]{:T(128)} %constant.83.clone.1..sunk, s32[]{:T(128)} %constant.83.clone.1..sunk, s32[]{:T(128)} %constant.83.clone.1..sunk) | dynamic-update-slice | bytes 524292 | tf_op jit(solution)/shard_map/while/body/jit(dynamic_update_index_in_dim)/dynamic_update_slice | solution.py:144
  79.3 1.0 constant_dynamic-slice_fusion.10
  83.1 8.2 %dynamic_update_slice.19 = f32[8,128,2,256]{1,0,3,2:T(8,128)} dynamic-update-slice(f32[8,128,2,256]{1,0,3,2:T(8,128)} %get-tuple-element.661, f32[1,128,2,256]{1,0,3,2:T(1,128)S(1)} %copy.248, s32[]{:T(128)} %get-tuple-element.657, s32[]{:T(128)} %constant.83.clone.1..sunk, s32[]{:T(128)} %constant.83.clone.1..sunk, s32[]{:T(128)} %constant.83.clone.1..sunk) | dynamic-update-slice | bytes 524292 | tf_op jit(solution)/shard_map/while/body/jit(dynamic_update_index_in_dim)/dynamic_update_slice | solution.py:144
  96.3 8.2 %dynamic_update_slice.19 = f32[8,128,2,256]{1,0,3,2:T(8,128)} dynamic-update-slice(f32[8,128,2,256]{1,0,3,2:T(8,128)} %get-tuple-element.661, f32[1,128,2,256]{1,0,3,2:T(1,128)S(1)} %copy.248, s32[]{:T(128)} %get-tuple-element.657, s32[]{:T(128)} %constant.83.clone.1..sunk, s32[]{:T(128)} %constant.83.clone.1..sunk, s32[]{:T(128)} %constant.83.clone.1..sunk) | dynamic-update-slice | bytes 524292 | tf_op jit(solution)/shard_map/while/body/jit(dynamic_update_index_in_dim)/dynamic_update_slice | solution.py:144
  109.4 8.2 %dynamic_update_slice.19 = f32[8,128,2,256]{1,0,3,2:T(8,128)} dynamic-update-slice(f32[8,128,2,256]{1,0,3,2:T(8,128)} %get-tuple-element.661, f32[1,128,2,256]{1,0,3,2:T(1,128)S(1)} %copy.248, s32[]{:T(128)} %get-tuple-element.657, s32[]{:T(128)} %constant.83.clone.1..sunk, s32[]{:T(128)} %constant.83.clone.1..sunk, s32[]{:T(128)} %constant.83.clone.1..sunk) | dynamic-update-slice | bytes 524292 | tf_op jit(solution)/shard_map/while/body/jit(dynamic_update_index_in_dim)/dynamic_update_slice | solution.py:144
  122.2 22.3 %all-gather.3 = bf16[8,1,2]{2,1,0:T(2,128)(2,1)S(1)} all-gather(bf16[1,1,2]{2,1,0:T(2,128)(2,1)S(1)} %bitcast.273), channel_id=1, replica_groups=mesh['sp'=8,'tp'=4] {'sp'}, dimensions={0}, use_global_device_ids=true | all-gather | bytes 36 | tf_op jit(solution)/shard_map/all_gather | solution.py:14
  144.5 17.5 %all-reduce = bf16[16]{0:T(256)(128)(2,1)S(1)} all-reduce(bf16[16]{0:T(256)(128)(2,1)S(1)} %dynamic-update-slice), channel_id=2, replica_groups=mesh['sp'=8,'tp'=4] {'sp'}, use_global_device_ids=true, to_apply=%add | all-reduce | flops 16 | bytes 64
  162.2 1.2 copy.155
  163.5 1.3 copy.156
  164.8 1.7 reshape.187
  166.5 18.0 %all-gather.4 = bf16[8,2,128]{2,1,0:T(2,128)(2,1)S(1)} all-gather(bf16[1,2,128]{2,1,0:T(2,128)(2,1)S(1)} %convert_bitcast_fusion), channel_id=4, replica_groups=mesh['sp'=8,'tp'=4] {'sp'}, dimensions={0}, use_global_device_ids=true | all-gather | bytes 4608 | tf_op jit(solution)/shard_map/all_gather | solution.py:14
  184.5 10.5 %while.40 = (s32[]{:T(128)}, f32[2,256,128]{2,1,0:T(8,128)S(1)}, f32[2,128]{1,0:T(2,128)S(1)}, f32[2]{0:T(128)S(1)}, s32[]{:T(128)}, /*index=5*/bf16[8,2]{0,1:T(...) while((s32[]{:T(128)}, f32[2,256,128]{2,1,0:T(8,128)S(1)}, ...), condition=%wide.region_10.11_spmd.clone, body=%wide.region_9.10_spmd.clone.sunk | while | flops 394772 | bytes 658157 | solution.py:29
  184.7 1.0 fusion.107
  186.1 1.0 fusion.107
  187.4 1.0 fusion.107
  188.7 1.0 fusion.107
  190.0 1.0 fusion.107
  191.3 1.0 fusion.107
  192.6 1.0 fusion.107
  193.9 1.0 fusion.107
  195.1 1.0 fusion.52
  196.2 2.2 multiply_reduce_fusion
  198.7 1.9 copy.141
  200.6 2.5 multiply_convert_fusion
  203.1 26.9 %all_to_all.19 = bf16[4,256,512]{2,1,0:T(8,128)(2,1)S(1)} all-to-all(bf16[4,256,512]{2,1,0:T(8,128)(2,1)S(1)} %bitcast.262), channel_id=1, replica_groups=mesh['sp'=8,'tp'=4] {'tp'}, dimensions={0} | all-to-all | bytes 2097152 | tf_op jit(solution)/shard_map/all_to_all | solution.py:191
  230.5 5.7 fusion.45
  236.6 1.3 fusion.48
  239.9 33.9 %all-gather.14.cloned.1.call-done = bf16[1024,2048]{1,0:T(8,128)(2,1)} async-done(((bf16[256,2048]{1,0:T(8,128)(2,1)}), bf16[1024,2048]{1,0:T(8,128)(2,1)}) %all-gather.14.cloned.1.call-update) | async-done | bytes 4194320 | tf_op jit(solution)/shard_map/all_gather | solution.py:201
  274.6 3.4 collective-permute-start
  278.1 90.1 %all-gather.16.cloned.1.call-done = bf16[2048,1408]{1,0:T(8,128)(2,1)} async-done(((bf16[256,1408]{1,0:T(8,128)(2,1)}), bf16[2048,1408]{1,0:T(8,128)(2,1)}) %all-gather.16.cloned.1.call-update) | async-done | bytes 5767184 | tf_op jit(solution)/shard_map/all_gather | solution.py:206
  368.2 11.9 %fusion.44 = f32[1026,1408]{1,0:T(8,128)} fusion(bf16[2048,1408]{1,0:T(8,128)(2,1)} %all-gather.16.cloned.1.call-done, bf16[1024,2048]{1,0:T(8,128)(2,1)} %all-gather.14.cloned.1.call-done, bf16[2,2048]{1,0:T(2,128)(2,1)S(1)} %collective-permute-done), kind=kOutput, calls=%fused_computation.90 | convolution fusion | flops 5925519360 | bytes 15748096 | tf_op jit(solution)/shard_map/dot_general | solution.py:204
  380.1 80.6 %all-gather.18.cloned.1.call-done = bf16[2048,1408]{1,0:T(8,128)(2,1)} async-done(((bf16[256,1408]{1,0:T(8,128)(2,1)}), bf16[2048,1408]{1,0:T(8,128)(2,1)}) %all-gather.18.cloned.1.call-update) | async-done | bytes 5767184 | tf_op jit(solution)/shard_map/all_gather | solution.py:211
  460.7 11.9 %fusion.43 = f32[1026,1408]{1,0:T(8,128)} fusion(bf16[2048,1408]{1,0:T(8,128)(2,1)} %all-gather.18.cloned.1.call-done, bf16[1024,2048]{1,0:T(8,128)(2,1)} %all-gather.14.cloned.1.call-done, bf16[2,2048]{1,0:T(2,128)(2,1)S(1)} %collective-permute-done), kind=kOutput, calls=%fused_computation.89 | convolution fusion | flops 5925519360 | bytes 15748096 | tf_op jit(solution)/shard_map/dot_general | solution.py:209
  472.6 81.3 %all-gather.20.cloned.1.call-done = bf16[1408,2048]{1,0:T(8,128)(2,1)} async-done(((bf16[1408,256]{1,0:T(8,128)(2,1)}), bf16[1408,2048]{1,0:T(8,128)(2,1)}) %all-gather.20.cloned.1.call-update) | async-done | bytes 5767184 | tf_op jit(solution)/shard_map/all_gather | solution.py:225
  554.0 22.7 %convolution_convert_fusion = bf16[1024,2048]{1,0:T(8,128)(2,1)} fusion(bf16[1408,2048]{1,0:T(8,128)(2,1)} %all-gather.20.cloned.1.call-done, f32[1026,1408]{1,0:T(8,128)} %fusion.43, f32[1026,1408]{1,0:T(8,128)} %fusion.44, f32[1408]{0:T(1024)S(1)} %get-tuple-element.403, f32[1408]{0:T(1024)S(1)} %get-tuple-element.404, f32[1408]{0:T(1024)S(1)} %get-tuple-element.402, ...), kind=kOutput, calls=%fused_computation.85 | convolution fusion | flops 5930745856 | bytes 44598272 | tf_op jit(solution)/shard_map/dot_general | solution.py:227
  576.7 42.9 %reduce-scatter.2.cloned.1.call-done = bf16[256,2048]{1,0:T(8,128)(2,1)} async-done(((bf16[1024,2048]{1,0:T(8,128)(2,1)}), bf16[256,2048]{1,0:T(8,128)(2,1)}) %reduce-scatter.2.cloned.1.call-update) | async-done | bytes 1048592 | tf_op jit(solution)/shard_map/reduce_scatter | solution.py:226
  619.6 2.6 fusion.49
  (321 shorter events, 46.6 us)
Async XLA Ops:
  6.5 5.3 copy-start.1
  6.5 178.0 %all-gather.22.cloned.1.call-start = ((), (), s32[]{:S(2)}) async-start(), calls=%async_computation.8 | async-start | bytes 1179648 | tf_op jit(solution)/shard_map/all_gather | solution.py:14
  12.8 107.7 %copy-start.7 = (u32[32]{0:T(128)S(1)}, u32[32]{0:T(128)}, u32[]{:S(2)}) copy-start(u32[32]{0:T(128)} %constant.101) | copy-start | bytes 388
  118.7 111.8 %all-gather.12.cloned.1.call-start = ((), (), s32[]{:S(2)}) async-start(), calls=%async_computation.2 | async-start | bytes 10485760 | tf_op jit(solution)/shard_map/all_gather | solution.py:190
  119.4 154.4 %all-gather.14.cloned.1.call-start = ((), (), s32[]{:S(2)}) async-start(), calls=%async_computation.3 | async-start | bytes 5242880 | tf_op jit(solution)/shard_map/all_gather | solution.py:201
  163.5 31.6 %copy-start.2 = (bf16[1024,256]{1,0:T(8,128)(2,1)S(1)}, bf16[1024,256]{1,0:T(8,128)(2,1)}, u32[]{:S(2)}) copy-start(bf16[1024,256]{1,0:T(8,128)(2,1)} %param.21) | copy-start | bytes 1572868
  196.2 2.3 copy-start.6
  200.6 29.9 %copy-start = (bf16[256,2048]{1,0:T(8,128)(2,1)S(1)}, bf16[256,2048]{1,0:T(8,128)(2,1)}, u32[]{:S(2)}) copy-start(bf16[256,2048]{1,0:T(8,128)(2,1)} %param.20) | copy-start | bytes 3145732
  230.5 6.1 copy-start.5
  236.3 41.7 %copy-start.3 = (f32[3,1408]{1,0:T(4,128)S(1)}, f32[3,1408]{1,0:T(4,128)}, u32[]{:S(2)}) copy-start(f32[3,1408]{1,0:T(4,128)} %param.34) | copy-start | bytes 50692
  236.3 41.7 %copy-start.4 = (f32[3,1408]{1,0:T(4,128)S(1)}, f32[3,1408]{1,0:T(4,128)}, u32[]{:S(2)}) copy-start(f32[3,1408]{1,0:T(4,128)} %param.33) | copy-start | bytes 50692
  237.9 130.3 %all-gather.16.cloned.1.call-start = ((), (), s32[]{:S(2)}) async-start(), calls=%async_computation.4 | async-start | bytes 6488064 | tf_op jit(solution)/shard_map/all_gather | solution.py:206
  238.5 222.3 %all-gather.18.cloned.1.call-start = ((), (), s32[]{:S(2)}) async-start(), calls=%async_computation.5 | async-start | bytes 6488064 | tf_op jit(solution)/shard_map/all_gather | solution.py:211
  239.1 314.9 %all-gather.20.cloned.1.call-start = ((), (), s32[]{:S(2)}) async-start(), calls=%async_computation.6 | async-start | bytes 6488064 | tf_op jit(solution)/shard_map/all_gather | solution.py:225
  239.7 379.9 %reduce-scatter.2.cloned.1.call-start = ((), (), s32[]{:S(2)}) async-start(), calls=%async_computation.7 | async-start | bytes 5242880 | tf_op jit(solution)/shard_map/reduce_scatter | solution.py:226
  274.6 93.6 %collective-permute-start = (bf16[2,2048]{1,0:T(2,128)(2,1)S(1)}, bf16[2,2048]{1,0:T(2,128)(2,1)S(1)}, u32[]{:S(2)}, u32[]{:S(2)}) collective-permute-start(bf16[2,2048]{1,0:T(2,128)(2,1)S(1)} %slice.72), channel_id=1, source_target_pairs={{0,4},{4,8},{8,12},{12,16},{16,20},{20,24},{24,28},{1,5},{5,9},{9,... | collective-permute-start | bytes 24584 | tf_op jit(solution)/shard_map/ppermute | solution.py:35
Sparse Core Ops, SparseCore 0:
  118.8 43.2 all-gather.21
  163.6 66.6 all-gather.11
  238.0 35.7 all-gather.13
  275.8 92.3 all-gather.15
  370.2 90.4 all-gather.17
  462.6 91.2 all-gather.19
  576.8 42.7 reduce-scatter.1
where the time goes:
time: 631 us; the launch traced here: 629 us
  waiting for transfers between devices  331 us (52%)
  local copies, waits for them, and re-layouts  97.1 us (15%)
  blocking collectives  84.7 us (13%)
  matrix products  67.5 us (11%)
  other arithmetic  29.4 us (5%)
  between operations  14.4 us (2%)
    all_gather x1, waiting for transfers between devices, local(): lax.all_gather(gate_up_weight, 'sp', axis=0, tiled=True)  90.1 us
    all_gather x1, waiting for transfers between devices, local(): lax.all_gather(down_projection_weight, 'sp', axis=1, tiled=True)  81.3 us
    all_gather x1, waiting for transfers between devices, local(): lax.all_gather(value_up_weight, 'sp', axis=0, tiled=True)  80.6 us
    dynamic_update_slice x16, local copies, waits for them, and re-layouts, local(): lax.scan(local_step, initial, (blocks(queries_low), blocks(keys_low), blo...  66.7 us
    reduce_scatter x1, waiting for transfers between devices, local(): lax.psum_scatter(jnp.dot(hidden, whole_down, preferred_element_type=jnp.f...  42.9 us
    all_gather x2, blocking collectives, carried_in(): lax.all_gather(part.astype(kind), axis)  40.3 us
    all_gather x1, waiting for transfers between devices, local(): group_rows = lax.all_gather(normed_rows, 'tp', axis=0, tiled=True)  33.9 us
    all_to_all x1, blocking collectives, local(): lax.all_to_all(gated_rows, 'tp', split_axis=0, concat_axis=1, tiled=True)  26.9 us
  transfers between devices with their start and end apart: 8, of which 5 were waited for; matrix products, arithmetic and copies ran while one was open for 8% of the time, Pallas kernels for 0%

commit v1 on v0

--- a/solution.py
+++ b/solution.py
@@ -198,7 +198,14 @@
         * lax.rsqrt(jnp.mean(stream_wide * stream_wide, axis=-1, keepdims=True) + eps)
         * feedforward_norm_gain[None, :]
     ).astype(jnp.bfloat16)
-    group_rows = lax.all_gather(normed_rows, "tp", axis=0, tiled=True)
+    devices = lax.axis_size("tp")
+    right = [(i_2, (i_2 + 1) % devices) for i_2 in range(devices)]
+    terms = [normed_rows]
+    for far in range(1, devices):
+        terms = [lax.ppermute(terms[0], "tp", right), *terms]
+    out = jnp.concatenate(terms, axis=0)
+    offset = (lax.axis_index("tp") + 1) * terms[-1].shape[0]
+    group_rows = jnp.roll(out, offset, axis=0)
     earlier_rows = shifted(group_rows[-2:], "sp", 1)
     window = jnp.concatenate([earlier_rows, group_rows], axis=0)
     up_gate = jnp.dot(

time: 631 us -> 591 us (0.937)
  waiting for transfers between devices: 331 us -> 286 us
    all_gather x1, waiting for transfers between devices: 90.1 us -> 36.5 us  [local(): lax.all_gather(gate_up_weight, 'sp', axis=0, tiled=True)]
    ppermute x0 -> x3, waiting for transfers between devices: none -> 42.4 us  [local(): terms = [lax.ppermute(terms[0], 'tp', right), *terms]]
    all_gather x1 -> x0, waiting for transfers between devices: 33.9 us -> none  [local(): group_rows = lax.all_gather(normed_rows, 'tp', axis=0, tiled=True)]
  transfers between devices with their start and end apart: 8 -> 10, of which waited for: 5 -> 7; matrix products, arithmetic and copies ran while one was open for 8% -> 11% of each run, Pallas kernels for 0% -> 0%
where the time goes in v1:
time: 591 us; the launch traced here: 588 us
  waiting for transfers between devices  286 us (48%)
  local copies, waits for them, and re-layouts  103 us (17%)
  blocking collectives  83.4 us (14%)
  matrix products  67.5 us (11%)
  other arithmetic  29 us (5%)
  between operations  14.4 us (2%)
    all_gather x1, waiting for transfers between devices, local(): lax.all_gather(down_projection_weight, 'sp', axis=1, tiled=True)  81.3 us
    all_gather x1, waiting for transfers between devices, local(): lax.all_gather(value_up_weight, 'sp', axis=0, tiled=True)  80.7 us
    dynamic_update_slice x16, local copies, waits for them, and re-layouts, local(): lax.scan(local_step, initial, (blocks(queries_low), blocks(keys_low), blo...  66.7 us
    reduce_scatter x1, waiting for transfers between devices, local(): lax.psum_scatter(jnp.dot(hidden, whole_down, preferred_element_type=jnp.f...  42.9 us
    ppermute x3, waiting for transfers between devices, local(): terms = [lax.ppermute(terms[0], 'tp', right), *terms]  42.4 us
    all_gather x1, waiting for transfers between devices, local(): lax.all_gather(gate_up_weight, 'sp', axis=0, tiled=True)  36.5 us
    all_gather x2, blocking collectives, carried_in(): lax.all_gather(part.astype(kind), axis)  34.6 us
    all_to_all x1, blocking collectives, local(): lax.all_to_all(gated_rows, 'tp', split_axis=0, concat_axis=1, tiled=True)  25.5 us
  transfers between devices with their start and end apart: 10, of which 7 were waited for; matrix products, arithmetic and copies ran while one was open for 11% of the time, Pallas kernels for 0%

profile of v1, /device:TPU:0, one launch (start us, length us, event | category | flops | bytes accessed | tf_op | source)
XLA Modules:
  0.0 588.2 jit_solution(12758611576676642751)
XLA Ops:
  7.5 1.3 reshape.215
  9.8 2.0 reshape.216
  11.8 2.0 reshape.217
  13.8 105.2 %while.39 = (s32[]{:T(128)}, f32[2,256,128]{2,1,0:T(8,128)S(1)}, f32[2,128]{1,0:T(2,128)S(1)}, f32[2]{0:T(128)S(1)}, f32[8,128,2,256]{1,0,3,2:T(8,128)}, /*index...) while((s32[]{:T(128)}, f32[2,256,128]{2,1,0:T(8,128)S(1)}, ...), condition=%wide.region_6.7_spmd.clone, body=%wide.region_0.6_spmd.clone.sunk | while | flops 144166400 | bytes 4685610 | solution.py:144
  18.3 8.2 %dynamic_update_slice.19 = f32[8,128,2,256]{1,0,3,2:T(8,128)} dynamic-update-slice(f32[8,128,2,256]{1,0,3,2:T(8,128)} %get-tuple-element.661, f32[1,128,2,256]{1,0,3,2:T(1,128)S(1)} %copy.248, s32[]{:T(128)} %get-tuple-element.657, s32[]{:T(128)} %constant.105.clone.1..sunk, s32[]{:T(128)} %constant.105.clone.1..sunk, s32[]{:T(128)} %constant.105.clone.1..sunk) | dynamic-update-slice | bytes 524292 | tf_op jit(solution)/shard_map/while/body/jit(dynamic_update_index_in_dim)/dynamic_update_slice | solution.py:144
  31.5 8.2 %dynamic_update_slice.19 = f32[8,128,2,256]{1,0,3,2:T(8,128)} dynamic-update-slice(f32[8,128,2,256]{1,0,3,2:T(8,128)} %get-tuple-element.661, f32[1,128,2,256]{1,0,3,2:T(1,128)S(1)} %copy.248, s32[]{:T(128)} %get-tuple-element.657, s32[]{:T(128)} %constant.105.clone.1..sunk, s32[]{:T(128)} %constant.105.clone.1..sunk, s32[]{:T(128)} %constant.105.clone.1..sunk) | dynamic-update-slice | bytes 524292 | tf_op jit(solution)/shard_map/while/body/jit(dynamic_update_index_in_dim)/dynamic_update_slice | solution.py:144
  44.6 8.2 %dynamic_update_slice.19 = f32[8,128,2,256]{1,0,3,2:T(8,128)} dynamic-update-slice(f32[8,128,2,256]{1,0,3,2:T(8,128)} %get-tuple-element.661, f32[1,128,2,256]{1,0,3,2:T(1,128)S(1)} %copy.248, s32[]{:T(128)} %get-tuple-element.657, s32[]{:T(128)} %constant.105.clone.1..sunk, s32[]{:T(128)} %constant.105.clone.1..sunk, s32[]{:T(128)} %constant.105.clone.1..sunk) | dynamic-update-slice | bytes 524292 | tf_op jit(solution)/shard_map/while/body/jit(dynamic_update_index_in_dim)/dynamic_update_slice | solution.py:144
  57.8 8.2 %dynamic_update_slice.19 = f32[8,128,2,256]{1,0,3,2:T(8,128)} dynamic-update-slice(f32[8,128,2,256]{1,0,3,2:T(8,128)} %get-tuple-element.661, f32[1,128,2,256]{1,0,3,2:T(1,128)S(1)} %copy.248, s32[]{:T(128)} %get-tuple-element.657, s32[]{:T(128)} %constant.105.clone.1..sunk, s32[]{:T(128)} %constant.105.clone.1..sunk, s32[]{:T(128)} %constant.105.clone.1..sunk) | dynamic-update-slice | bytes 524292 | tf_op jit(solution)/shard_map/while/body/jit(dynamic_update_index_in_dim)/dynamic_update_slice | solution.py:144
  70.9 8.2 %dynamic_update_slice.19 = f32[8,128,2,256]{1,0,3,2:T(8,128)} dynamic-update-slice(f32[8,128,2,256]{1,0,3,2:T(8,128)} %get-tuple-element.661, f32[1,128,2,256]{1,0,3,2:T(1,128)S(1)} %copy.248, s32[]{:T(128)} %get-tuple-element.657, s32[]{:T(128)} %constant.105.clone.1..sunk, s32[]{:T(128)} %constant.105.clone.1..sunk, s32[]{:T(128)} %constant.105.clone.1..sunk) | dynamic-update-slice | bytes 524292 | tf_op jit(solution)/shard_map/while/body/jit(dynamic_update_index_in_dim)/dynamic_update_slice | solution.py:144
  84.1 8.2 %dynamic_update_slice.19 = f32[8,128,2,256]{1,0,3,2:T(8,128)} dynamic-update-slice(f32[8,128,2,256]{1,0,3,2:T(8,128)} %get-tuple-element.661, f32[1,128,2,256]{1,0,3,2:T(1,128)S(1)} %copy.248, s32[]{:T(128)} %get-tuple-element.657, s32[]{:T(128)} %constant.105.clone.1..sunk, s32[]{:T(128)} %constant.105.clone.1..sunk, s32[]{:T(128)} %constant.105.clone.1..sunk) | dynamic-update-slice | bytes 524292 | tf_op jit(solution)/shard_map/while/body/jit(dynamic_update_index_in_dim)/dynamic_update_slice | solution.py:144
  97.2 8.2 %dynamic_update_slice.19 = f32[8,128,2,256]{1,0,3,2:T(8,128)} dynamic-update-slice(f32[8,128,2,256]{1,0,3,2:T(8,128)} %get-tuple-element.661, f32[1,128,2,256]{1,0,3,2:T(1,128)S(1)} %copy.248, s32[]{:T(128)} %get-tuple-element.657, s32[]{:T(128)} %constant.105.clone.1..sunk, s32[]{:T(128)} %constant.105.clone.1..sunk, s32[]{:T(128)} %constant.105.clone.1..sunk) | dynamic-update-slice | bytes 524292 | tf_op jit(solution)/shard_map/while/body/jit(dynamic_update_index_in_dim)/dynamic_update_slice | solution.py:144
  110.4 8.2 %dynamic_update_slice.19 = f32[8,128,2,256]{1,0,3,2:T(8,128)} dynamic-update-slice(f32[8,128,2,256]{1,0,3,2:T(8,128)} %get-tuple-element.661, f32[1,128,2,256]{1,0,3,2:T(1,128)S(1)} %copy.248, s32[]{:T(128)} %get-tuple-element.657, s32[]{:T(128)} %constant.105.clone.1..sunk, s32[]{:T(128)} %constant.105.clone.1..sunk, s32[]{:T(128)} %constant.105.clone.1..sunk) | dynamic-update-slice | bytes 524292 | tf_op jit(solution)/shard_map/while/body/jit(dynamic_update_index_in_dim)/dynamic_update_slice | solution.py:144
  123.3 23.3 %all-reduce = bf16[16]{0:T(256)(128)(2,1)S(1)} all-reduce(bf16[16]{0:T(256)(128)(2,1)S(1)} %dynamic-update-slice), channel_id=2, replica_groups=mesh['sp'=8,'tp'=4] {'sp'}, use_global_device_ids=true, to_apply=%add | all-reduce | flops 16 | bytes 64
  146.7 16.4 %all-gather.4 = bf16[8,2,128]{2,1,0:T(2,128)(2,1)S(1)} all-gather(bf16[1,2,128]{2,1,0:T(2,128)(2,1)S(1)} %convert_bitcast_fusion), channel_id=4, replica_groups=mesh['sp'=8,'tp'=4] {'sp'}, dimensions={0}, use_global_device_ids=true | all-gather | bytes 4608 | tf_op jit(solution)/shard_map/all_gather | solution.py:14
  164.3 18.2 %all-gather.3 = bf16[8,1,2]{2,1,0:T(2,128)(2,1)S(1)} all-gather(bf16[1,1,2]{2,1,0:T(2,128)(2,1)S(1)} %bitcast.275), channel_id=1, replica_groups=mesh['sp'=8,'tp'=4] {'sp'}, dimensions={0}, use_global_device_ids=true | all-gather | bytes 36 | tf_op jit(solution)/shard_map/all_gather | solution.py:14
  182.6 1.2 copy.155
  183.9 1.2 copy.156
  185.1 1.7 reshape.187
  186.9 10.5 %while.40 = (s32[]{:T(128)}, f32[2,256,128]{2,1,0:T(8,128)S(1)}, f32[2,128]{1,0:T(2,128)S(1)}, f32[2]{0:T(128)S(1)}, s32[]{:T(128)}, /*index=5*/bf16[8,2]{0,1:T(...) while((s32[]{:T(128)}, f32[2,256,128]{2,1,0:T(8,128)S(1)}, ...), condition=%wide.region_10.11_spmd.clone, body=%wide.region_9.10_spmd.clone.sunk | while | flops 394772 | bytes 658157 | solution.py:29
  187.1 1.0 fusion.107
  188.4 1.0 fusion.107
  189.7 1.0 fusion.107
  191.0 1.0 fusion.107
  192.3 1.0 fusion.107
  193.6 1.0 fusion.107
  195.0 1.0 fusion.107
  196.3 1.0 fusion.107
  197.4 1.0 fusion.52
  198.5 2.2 multiply_reduce_fusion
  201.1 1.9 copy.141
  202.9 2.5 multiply_convert_fusion
  205.5 25.5 %all_to_all.19 = bf16[4,256,512]{2,1,0:T(8,128)(2,1)S(1)} all-to-all(bf16[4,256,512]{2,1,0:T(8,128)(2,1)S(1)} %bitcast.262), channel_id=1, replica_groups=mesh['sp'=8,'tp'=4] {'tp'}, dimensions={0} | all-to-all | bytes 2097152 | tf_op jit(solution)/shard_map/all_to_all | solution.py:191
  231.5 5.7 fusion.45
  238.2 14.0 %collective-permute-done = bf16[256,2048]{1,0:T(8,128)(2,1)S(1)} collective-permute-done((bf16[256,2048]{1,0:T(8,128)(2,1)S(1)}, bf16[256,2048]{1,0:T(8,128)(2,1)S(1)}, u32[]{:S(2)}, u32[]{:S(2)}) %collective-permute-start) | collective-permute-done | bytes 1048608 | tf_op jit(solution)/shard_map/ppermute | solution.py:205
  252.1 14.2 %collective-permute-done.1 = bf16[256,2048]{1,0:T(8,128)(2,1)S(1)} collective-permute-done((bf16[256,2048]{1,0:T(8,128)(2,1)S(1)}, bf16[256,2048]{1,0:T(8,128)(2,1)S(1)}, u32[]{:S(2)}, u32[]{:S(2)}) %collective-permute-start.1) | collective-permute-done | bytes 1048608 | tf_op jit(solution)/shard_map/ppermute | solution.py:205
  266.5 14.2 %collective-permute-done.2 = bf16[256,2048]{1,0:T(8,128)(2,1)} collective-permute-done((bf16[256,2048]{1,0:T(8,128)(2,1)S(1)}, bf16[256,2048]{1,0:T(8,128)(2,1)}, u32[]{:S(2)}, u32[]{:S(2)}) %collective-permute-start.2) | collective-permute-done | bytes 1048608 | tf_op jit(solution)/shard_map/ppermute | solution.py:205
  280.7 1.3 constant_dynamic-update-slice_fusion.7
  282.5 1.3 constant_dynamic-update-slice_fusion.3
  284.3 3.4 collective-permute-start.3
  287.7 3.2 constant_dynamic-slice_fusion.7
  290.9 36.5 %all-gather.13.cloned.1.call-done = bf16[2048,1408]{1,0:T(8,128)(2,1)} async-done(((bf16[256,1408]{1,0:T(8,128)(2,1)}), bf16[2048,1408]{1,0:T(8,128)(2,1)}) %all-gather.13.cloned.1.call-update) | async-done | bytes 5767184 | tf_op jit(solution)/shard_map/all_gather | solution.py:213
  327.4 11.9 %fusion.44 = f32[1026,1408]{1,0:T(8,128)} fusion(bf16[2048,1408]{1,0:T(8,128)(2,1)} %all-gather.13.cloned.1.call-done, bf16[1024,2048]{1,0:T(8,128)(2,1)} %constant_dynamic-slice_fusion.7, bf16[2,2048]{1,0:T(2,128)(2,1)S(1)} %collective-permute-done.3), kind=kOutput, calls=%fused_computation.90 | convolution fusion | flops 5925519360 | bytes 15748096 | tf_op jit(solution)/shard_map/dot_general | solution.py:211
  339.3 80.7 %all-gather.15.cloned.1.call-done = bf16[2048,1408]{1,0:T(8,128)(2,1)} async-done(((bf16[256,1408]{1,0:T(8,128)(2,1)}), bf16[2048,1408]{1,0:T(8,128)(2,1)}) %all-gather.15.cloned.1.call-update) | async-done | bytes 5767184 | tf_op jit(solution)/shard_map/all_gather | solution.py:218
  420.0 11.9 %fusion.43 = f32[1026,1408]{1,0:T(8,128)} fusion(bf16[2048,1408]{1,0:T(8,128)(2,1)} %all-gather.15.cloned.1.call-done, bf16[1024,2048]{1,0:T(8,128)(2,1)} %constant_dynamic-slice_fusion.7, bf16[2,2048]{1,0:T(2,128)(2,1)S(1)} %collective-permute-done.3), kind=kOutput, calls=%fused_computation.89 | convolution fusion | flops 5925519360 | bytes 15748096 | tf_op jit(solution)/shard_map/dot_general | solution.py:216
  431.9 81.3 %all-gather.17.cloned.1.call-done = bf16[1408,2048]{1,0:T(8,128)(2,1)} async-done(((bf16[1408,256]{1,0:T(8,128)(2,1)}), bf16[1408,2048]{1,0:T(8,128)(2,1)}) %all-gather.17.cloned.1.call-update) | async-done | bytes 5767184 | tf_op jit(solution)/shard_map/all_gather | solution.py:232
  513.2 22.7 %convolution_convert_fusion = bf16[1024,2048]{1,0:T(8,128)(2,1)} fusion(bf16[1408,2048]{1,0:T(8,128)(2,1)} %all-gather.17.cloned.1.call-done, f32[1026,1408]{1,0:T(8,128)} %fusion.43, f32[1026,1408]{1,0:T(8,128)} %fusion.44, f32[1408]{0:T(1024)S(1)} %get-tuple-element.403, f32[1408]{0:T(1024)S(1)} %get-tuple-element.404, f32[1408]{0:T(1024)S(1)} %get-tuple-element.402, ...), kind=kOutput, calls=%fused_computation.85 | convolution fusion | flops 5930745856 | bytes 44598272 | tf_op jit(solution)/shard_map/dot_general | solution.py:234
  535.9 42.9 %reduce-scatter.2.cloned.1.call-done = bf16[256,2048]{1,0:T(8,128)(2,1)} async-done(((bf16[1024,2048]{1,0:T(8,128)(2,1)}), bf16[256,2048]{1,0:T(8,128)(2,1)}) %reduce-scatter.2.cloned.1.call-update) | async-done | bytes 1048592 | tf_op jit(solution)/shard_map/reduce_scatter | solution.py:233
  578.8 2.6 fusion.49
  (331 shorter events, 50.7 us)
Async XLA Ops:
  6.5 180.3 %all-gather.19.cloned.1.call-start = ((), (), s32[]{:S(2)}) async-start(), calls=%async_computation.7 | async-start | bytes 1179648 | tf_op jit(solution)/shard_map/all_gather | solution.py:14
  13.8 108.1 %copy-start.6 = (u32[32]{0:T(128)S(1)}, u32[32]{0:T(128)}, u32[]{:S(2)}) copy-start(u32[32]{0:T(128)} %constant.129) | copy-start | bytes 388
  119.7 77.7 %copy-start.1 = (bf16[1024,256]{1,0:T(8,128)(2,1)S(1)}, bf16[1024,256]{1,0:T(8,128)(2,1)}, u32[]{:S(2)}) copy-start(bf16[1024,256]{1,0:T(8,128)(2,1)} %param.21) | copy-start | bytes 1572868
  119.7 111.8 %all-gather.11.cloned.1.call-start = ((), (), s32[]{:S(2)}) async-start(), calls=%async_computation.2 | async-start | bytes 10485760 | tf_op jit(solution)/shard_map/all_gather | solution.py:190
  120.4 207.0 %all-gather.13.cloned.1.call-start = ((), (), s32[]{:S(2)}) async-start(), calls=%async_computation.3 | async-start | bytes 6488064 | tf_op jit(solution)/shard_map/all_gather | solution.py:213
  121.2 298.8 %all-gather.15.cloned.1.call-start = ((), (), s32[]{:S(2)}) async-start(), calls=%async_computation.4 | async-start | bytes 6488064 | tf_op jit(solution)/shard_map/all_gather | solution.py:218
  121.8 391.4 %all-gather.17.cloned.1.call-start = ((), (), s32[]{:S(2)}) async-start(), calls=%async_computation.5 | async-start | bytes 6488064 | tf_op jit(solution)/shard_map/all_gather | solution.py:232
  197.4 3.4 copy-start.5
  201.0 30.4 %copy-start = (bf16[256,2048]{1,0:T(8,128)(2,1)S(1)}, bf16[256,2048]{1,0:T(8,128)(2,1)}, u32[]{:S(2)}) copy-start(bf16[256,2048]{1,0:T(8,128)(2,1)} %param.20) | copy-start | bytes 3145732
  231.5 6.1 %copy-start.2 = (f32[2048]{0:T(1024)S(1)}, f32[2048]{0:T(1024)}, u32[]{:S(2)}) copy-start(f32[2048]{0:T(1024)} %param.30) | copy-start | bytes 24580
  231.5 34.9 %copy-start.3 = (f32[3,1408]{1,0:T(4,128)S(1)}, f32[3,1408]{1,0:T(4,128)}, u32[]{:S(2)}) copy-start(f32[3,1408]{1,0:T(4,128)} %param.34) | copy-start | bytes 50692
  231.5 34.9 %copy-start.4 = (f32[3,1408]{1,0:T(4,128)S(1)}, f32[3,1408]{1,0:T(4,128)}, u32[]{:S(2)}) copy-start(f32[3,1408]{1,0:T(4,128)} %param.33) | copy-start | bytes 50692
  237.9 14.3 %collective-permute-start = (bf16[256,2048]{1,0:T(8,128)(2,1)S(1)}, bf16[256,2048]{1,0:T(8,128)(2,1)S(1)}, u32[]{:S(2)}, u32[]{:S(2)}) collective-permute-start(bf16[256,2048]{1,0:T(8,128)(2,1)S(1)} %fusion.48), channel_id=1, source_target_pairs={{0,1},{1,2},{2,3},{3,0},{4,5},{5,6},{6,7},{7,4},{8,9},{9,10},{10,1... | collective-permute-start | bytes 3145736 | tf_op jit(solution)/shard_map/ppermute | solution.py:205
  238.0 340.9 %reduce-scatter.2.cloned.1.call-start = ((), (), s32[]{:S(2)}) async-start(), calls=%async_computation.6 | async-start | bytes 5242880 | tf_op jit(solution)/shard_map/reduce_scatter | solution.py:233
  252.1 14.2 %collective-permute-start.1 = (bf16[256,2048]{1,0:T(8,128)(2,1)S(1)}, bf16[256,2048]{1,0:T(8,128)(2,1)S(1)}, u32[]{:S(2)}, u32[]{:S(2)}) collective-permute-start(bf16[256,2048]{1,0:T(8,128)(2,1)S(1)} %collective-permute-done), channel_id=1, source_target_pairs={{0,1},{1,2},{2,3},{3,0},{4,5},{5,6},{6,7},{7,4},{8,9},{9,10},{10,1... | collective-permute-start | bytes 3145736 | tf_op jit(solution)/shard_map/ppermute | solution.py:205
  266.4 14.3 %collective-permute-start.2 = (bf16[256,2048]{1,0:T(8,128)(2,1)S(1)}, bf16[256,2048]{1,0:T(8,128)(2,1)}, u32[]{:S(2)}, u32[]{:S(2)}) collective-permute-start(bf16[256,2048]{1,0:T(8,128)(2,1)S(1)} %collective-permute-done.1), channel_id=1, source_target_pairs={{0,1},{1,2},{2,3},{3,0},{4,5},{5,6},{6,7},{7,4},{8,9},{9,10},{10,1... | collective-permute-start | bytes 3145736 | tf_op jit(solution)/shard_map/ppermute | solution.py:205
  284.3 43.1 %collective-permute-start.3 = (bf16[2,2048]{1,0:T(2,128)(2,1)S(1)}, bf16[2,2048]{1,0:T(2,128)(2,1)S(1)}, u32[]{:S(2)}, u32[]{:S(2)}) collective-permute-start(bf16[2,2048]{1,0:T(2,128)(2,1)S(1)} %constant_dynamic-slice_fusion.6), channel_id=1, source_target_pairs={{0,4},{4,8},{8,12},{12,16},{16,20},{20,24},{24,28},{1,5},{5,9},{9,... | collective-permute-start | bytes 24584 | tf_op jit(solution)/shard_map/ppermute | solution.py:35
Sparse Core Ops, SparseCore 0:
  119.8 43.0 all-gather.18
  164.5 65.4 all-gather.10
  232.2 95.1 all-gather.12
  329.4 90.4 all-gather.14
  421.9 91.3 all-gather.16
  536.0 42.7 reduce-scatter.1
